TPU v7x, 512 devices: a 8x2x16 block of a 8x16x16 slice. The times are simulated.
512 devices in a mesh: grp: 2 (over y), ep: 16 (over z), tp: 16 (over x, core).
Axes of the slice: x: 8, y: 2, z: 16, core: 2. Of those that a mesh axis runs over, the one named last changes fastest.
The devices are a block of a 8x16x16 slice.
Arguments:
- queries: bfloat16 [8192, 2048], P(('grp', 'ep'), 'tp'), parts along dimension 0, may hold values from -8 to 8
- keys: bfloat16 [8192, 512], P(('grp', 'ep')), parts along dimension 0, may hold values from -8 to 8
- values: bfloat16 [8192, 512], P(('grp', 'ep')), parts along dimension 0, may hold values from -6 to 6
- q_gain: float32 [128], replicated, may hold values from 0.6 to 5.8
- k_gain: float32 [128], replicated, may hold values from 0.6 to 5.8
- w_out: bfloat16 [2048, 2048], P(None, 'tp'), may hold values from -0.125 to 0.125
- moe_rows: bfloat16 [6144, 2048], P(('grp', 'ep')), parts along dimension 0, may hold values from -6 to 6
- routes: int32 [6144, 2], P(('grp', 'ep')), parts along dimension 0, may hold values from 0 to 15, all different within a row; in each aligned block of 192 rows (0 to 191, 192 to 383, ...) at most 36 rows name the same one
- group_gate: float32 [6144], P(('grp', 'ep')), parts along dimension 0, may hold values from 0.25 to 1
- expert_logits: float32 [6144, 2], P(('grp', 'ep')), parts along dimension 0, may hold values from -6 to 6
- moe_gain: float32 [2048], replicated, may hold values from 0.1 to 1.9
- w_gate: bfloat16 [16, 2048, 2048], P('ep', None, 'tp'), may hold values from -0.125 to 0.125
- w_up: bfloat16 [16, 2048, 2048], P('ep', None, 'tp'), may hold values from -0.125 to 0.125
- w_down: bfloat16 [16, 2048, 2048], P('ep', 'tp'), may hold values from -0.125 to 0.125
Outputs:
- attn_out: bfloat16 [8192, 2048], P(('grp', 'ep'), 'tp'), parts along dimension 0
- moe_out: bfloat16 [6144, 2048], P(('grp', 'ep'), 'tp'), parts along dimension 0
There are 2 independent parts, one for each index of `grp`. A program takes and returns all parts, laid end to end along the dimension named above; an argument that names none is the same for every part. Nothing has to cross between parts.
Inputs may be any that keep to these rules, and one draw needn't show every extreme that they name: `routes`: each row names 2 different experts; within the rows of one index of ep no expert is named more than 36 times, a bound that some block reaches.
All inputs are finite; a program needn't handle non-finite values.
Results may differ from a plain program's by a relative error of at most 0.019.
The roundings to bfloat16 on the way count: a program that leaves them out, or rounds other values in their place, can miss the bound.
Values may be sent and summed in bfloat16 or wider, within the bound.
A program may use at most 64 MiB of HBM per device.

v0:
```python
import jax
import jax.numpy as jnp
from jax import lax
from jax.sharding import PartitionSpec as P

HEADS = 16
KV_HEADS = 4
HEAD_DIM = 128
GRID_W = 64
TOPK = 2


def in_one_piece(arrays, axis, dim, along):
    both = jnp.concatenate(arrays, axis=along)
    result, at, finished = (lax.all_gather(both, axis, axis=dim, tiled=True), 0, [])
    for a in arrays:
        finished.append(lax.slice_in_dim(result, at, at + a.shape[along], axis=along))
        at += a.shape[along]
    return tuple(finished)


def laid_out(blocks, dim):
    blocks = jnp.moveaxis(blocks, 0, dim)
    shape = blocks.shape
    return blocks.reshape(*shape[:dim], shape[dim] * shape[dim + 1], *shape[dim + 2 :])


def copy_for_each(x, axis):
    copies = jnp.broadcast_to(x, (lax.axis_size(axis), *x.shape))
    return lax.all_to_all(copies, axis, split_axis=0, concat_axis=0, tiled=True)


def gather_directly(x, axis, dim):
    return laid_out(copy_for_each(x, axis), dim)


def in_blocks(x, dim, devices):
    before, after = (x.shape[:dim], x.shape[dim + 1 :])
    return jnp.moveaxis(x.reshape(*before, devices, -1, *after), dim, 0)


def sent_and_summed(x, axis, dim):
    blocks = in_blocks(x, dim, lax.axis_size(axis))
    arrived = lax.all_to_all(blocks, axis, split_axis=0, concat_axis=0, tiled=True)
    return arrived.astype(jnp.float32).sum(axis=0)


def head_norm(x, gain):
    wide = x.astype(jnp.float32)
    return wide * lax.rsqrt(jnp.mean(wide * wide, axis=-1, keepdims=True) + 1e-06) * gain


def rotate(x, first):
    count = x.shape[0]
    pos = first + jnp.arange(count, dtype=jnp.int32)
    row = (pos // GRID_W).astype(jnp.float32)
    col = (pos % GRID_W).astype(jnp.float32)
    nfreq = HEAD_DIM // 4
    inverse = 10000.0 ** (-jnp.arange(nfreq, dtype=jnp.float32) / nfreq)
    angle = jnp.concatenate(
        [
            row[:, None] * inverse,
            row[:, None] * inverse,
            col[:, None] * inverse,
            col[:, None] * inverse,
        ],
        axis=1,
    )
    parts = x.reshape(x.shape[:-1] + (2, 2, nfreq))
    turned = jnp.stack([-parts[..., 1, :], parts[..., 0, :]], axis=-2).reshape(x.shape)
    return x * jnp.cos(angle)[:, None, :] + turned * jnp.sin(angle)[:, None, :]


def per_device(
    queries,
    keys,
    values,
    q_gain,
    k_gain,
    w_out,
    moe_rows,
    routes,
    group_gate,
    expert_logits,
    moe_gain,
    w_gate,
    w_up,
    w_down,
):
    rows = queries.shape[0]
    heads_dev = queries.shape[1] // HEAD_DIM
    group = HEADS // KV_HEADS
    kv_dev = max(1, heads_dev // group)
    per_kv = heads_dev // kv_dev
    first_kv = lax.axis_index("tp") * heads_dev // group
    first_row = lax.axis_index("ep") * rows
    k_mine = lax.dynamic_slice_in_dim(keys, first_kv * HEAD_DIM, kv_dev * HEAD_DIM, 1)
    v_mine = lax.dynamic_slice_in_dim(values, first_kv * HEAD_DIM, kv_dev * HEAD_DIM, 1)
    k_rot = rotate(head_norm(k_mine.reshape(rows, kv_dev, HEAD_DIM), k_gain), first_row)
    k_rot = k_rot.astype(jnp.bfloat16).reshape(rows, kv_dev * HEAD_DIM)
    q_rot = rotate(head_norm(queries.reshape(rows, heads_dev, HEAD_DIM), q_gain), first_row)
    q_rot = q_rot.astype(jnp.bfloat16).reshape(rows, kv_dev, per_kv, HEAD_DIM)
    scale = HEAD_DIM ** (-0.5)
    top = jnp.full((rows, kv_dev, per_kv), -jnp.inf, jnp.float32)
    total = jnp.zeros((rows, kv_dev, per_kv), jnp.float32)
    acc = jnp.zeros((rows, kv_dev, per_kv, HEAD_DIM), jnp.float32)
    k_piece, v_piece = in_one_piece((k_rot, v_mine), "ep", 0, 1)
    count = k_piece.shape[0]
    key_rows = k_piece.reshape(count, kv_dev, HEAD_DIM)
    value_rows = v_piece.reshape(count, kv_dev, HEAD_DIM)
    scores = (
        jnp.einsum("qkgd,nkd->qkgn", q_rot, key_rows, preferred_element_type=jnp.float32) * scale
    )
    new_top = jnp.max(scores, axis=-1)
    shrink = jnp.exp(top - new_top)
    expo = jnp.exp(scores - new_top[..., None])
    total = total * shrink + jnp.sum(expo, axis=-1)
    acc = acc * shrink[..., None] + jnp.einsum(
        "qkgn,nkd->qkgd", expo.astype(jnp.bfloat16), value_rows, preferred_element_type=jnp.float32
    )
    top, total, acc = (new_top, total, acc)
    mixed = (acc / total[..., None]).astype(jnp.bfloat16).reshape(rows, heads_dev * HEAD_DIM)
    attn_out = jnp.dot(
        lax.all_gather(mixed, "tp", axis=1, tiled=True), w_out, preferred_element_type=jnp.float32
    ).astype(jnp.bfloat16)
    count = moe_rows.shape[0]
    width = moe_rows.shape[1]
    peers = lax.axis_size("ep")
    capacity = 3 * count // peers
    wide = moe_rows.astype(jnp.float32)
    normed = (
        wide * lax.rsqrt(jnp.mean(wide * wide, axis=-1, keepdims=True) + 1e-06) * moe_gain
    ).astype(jnp.bfloat16)
    chosen = routes.reshape(-1)
    onehot = (chosen[:, None] == jnp.arange(peers, dtype=jnp.int32)[None, :]).astype(jnp.int32)
    rank = jnp.sum((jnp.cumsum(onehot, axis=0) - onehot) * onehot, axis=1)
    slots = chosen * capacity + rank
    owner = jnp.arange(count * TOPK, dtype=jnp.int32) // TOPK
    source = jnp.zeros((peers * capacity,), jnp.int32).at[slots].set(owner)
    used = jnp.zeros((peers * capacity,), jnp.bool_).at[slots].set(True)
    outgoing = jnp.where(used[:, None], normed[source], jnp.zeros((), jnp.bfloat16)).reshape(
        peers, capacity, width
    )
    part_cols = width // lax.axis_size("tp")
    mine = lax.dynamic_slice_in_dim(outgoing, lax.axis_index("tp") * part_cols, part_cols, 2)
    arrived = gather_directly(
        lax.all_to_all(mine, "ep", split_axis=0, concat_axis=0, tiled=True), "tp", 2
    )
    first_dim, second_dim, cols = arrived.shape
    flat = arrived.reshape(first_dim * second_dim, cols)
    gate = jnp.dot(flat, w_gate[0], preferred_element_type=jnp.float32)
    up = jnp.dot(flat, w_up[0], preferred_element_type=jnp.float32)
    hidden = (jax.nn.silu(gate) * up).astype(jnp.bfloat16)
    result = jnp.dot(hidden, w_down[0], preferred_element_type=jnp.float32).astype(jnp.bfloat16)
    partial_value = result.reshape(first_dim, second_dim, cols)
    summed = sent_and_summed(partial_value, "tp", 2).astype(jnp.bfloat16)
    back = lax.all_to_all(summed, "ep", split_axis=0, concat_axis=0, tiled=True)
    back = back.reshape(peers * capacity, back.shape[2])
    picked = back[slots].astype(jnp.float32).reshape(count, TOPK, back.shape[1])
    weights = group_gate[:, None] * jax.nn.softmax(expert_logits, axis=-1)
    moe_out = jnp.sum(weights[:, :, None] * picked, axis=1).astype(jnp.bfloat16)
    return (attn_out, moe_out)


def solution(mesh):
    placed = (
        P(("grp", "ep"), "tp"),
        P(("grp", "ep"), None),
        P(("grp", "ep"), None),
        P(),
        P(),
        P(None, "tp"),
        P(("grp", "ep"), None),
        P(("grp", "ep"), None),
        P(("grp", "ep")),
        P(("grp", "ep"), None),
        P(),
        P("ep", None, "tp"),
        P("ep", None, "tp"),
        P("ep", "tp", None),
    )
    return jax.shard_map(
        per_device,
        mesh=mesh,
        in_specs=placed,
        out_specs=(P(("grp", "ep"), "tp"), P(("grp", "ep"), "tp")),
        check_vma=False,
    )
```

profile of v0, /device:TPU:80, one launch (start us, length us, event | category | flops | bytes accessed | tf_op | source)
XLA Modules:
  0.0 255.7 jit_solution(3186718910056621887)
XLA Ops:
  10.6 2.9 %scatter_custom_fusion.1 = s32[576]{0:T(1024)S(1)} fusion(s32[384]{0:T(512)S(1)} %fusion.75, s32[384]{0:T(512)S(1)} %add_select_fusion, s32[]{:T(128)} %constant.94.clone.1), kind=kCustom, calls=%fused_computation.92 | custom fusion | bytes 2308 | tf_op jit(solution)/shard_map/scatter | solution.py:139
  14.9 1.4 fusion.16
  16.3 4.0 %gather_fusion = bf16[576,2048]{1,0:T(8,128)(2,1)} fusion(bf16[192,2048]{1,0:T(8,128)(2,1)S(1)} %fusion.16, s32[1024]{0:T(1024)S(1)} %pad_clamp_fusion.1), kind=kCustom, calls=%fused_computation | custom fusion | bytes 4720896 | tf_op jit(solution)/shard_map/gather | solution.py:141
  20.3 2.6 %gather.9 = bf16[16,36,2048]{2,1,0:T(8,128)(2,1)S(1)} reshape(bf16[576,2048]{1,0:T(8,128)(2,1)} %gather_fusion) | data formatting | bytes 4718592 | tf_op jit(solution)/shard_map/gather | solution.py:141
  22.9 2.0 scatter_custom_fusion
  25.8 43.7 %all-to-all-start = ((bf16[16,36,128]{2,1,0:T(8,128)(2,1)}), bf16[16,36,128]{2,1,0:T(8,128)(2,1)S(1)}, u32[]{:S(2)}, u32[]{:S(2)}) async-start(bf16[16,36,128]{2,1,0:T(8,128)(2,1)} %dynamic-slice_select_fusion), calls=%async_computation | async-start | bytes 327680 | tf_op jit(solution)/shard_map/all_to_all | solution.py:147
  69.5 15.3 %all-to-all-done = bf16[16,36,128]{2,1,0:T(8,128)(2,1)S(1)} async-done(((bf16[16,36,128]{2,1,0:T(8,128)(2,1)}), bf16[16,36,128]{2,1,0:T(8,128)(2,1)S(1)}, u32[]{:S(2)}, u32[]{:S(2)}) %all-to-all-start) | async-done | bytes 147488 | tf_op jit(solution)/shard_map/all_to_all | solution.py:147
  84.9 1.9 broadcast_in_dim.30
  86.7 7.8 %all-to-all-start.1 = ((bf16[16,16,36,128]{3,1,2,0:T(8,128)(2,1)}), bf16[16,16,36,128]{3,1,2,0:T(8,128)(2,1)S(1)}, u32[]{:S(2)}, u32[]{:S(2)}) async-start(bf16[16,16,36,128]{3,1,2,0:T(8,128)(2,1)} %broadcast_in_dim.30), calls=%async_computation.1 | async-start | bytes 4718592 | tf_op jit(solution)/shard_map/all_to_all | solution.py:30
  97.5 51.7 %all-to-all-done.1 = bf16[16,16,36,128]{3,1,2,0:T(8,128)(2,1)S(1)} async-done(((bf16[16,16,36,128]{3,1,2,0:T(8,128)(2,1)}), bf16[16,16,36,128]{3,1,2,0:T(8,128)(2,1)S(1)}, u32[]{:S(2)}, u32[]{:S(2)}) %all-to-all-start.1) | async-done | bytes 2359328 | tf_op jit(solution)/shard_map/all_to_all | solution.py:30
  149.2 1.5 copy.67
  150.8 1.4 copy-done.1
  152.2 1.5 fusion.5
  153.7 4.2 %fusion.13 = bf16[72,8,16,128]{3,1,2,0:T(8,128)(2,1)S(1)} fusion(bf16[72,8,16,128]{3,2,1,0:T(8,128)(2,1)} %bitcast.124, bf16[1,128,2048]{2,1,0:T(8,128)(2,1)S(1)} %copy-done, bf16[1,2048,128]{2,1,0:T(8,128)(2,1)S(1)} %copy-done.3, f32[576,128]{1,0:T(8,128)} %fusion.5), kind=kOutput, calls=%fused_computation.22 | convolution fusion | flops 605601792 | bytes 6062080 | tf_op jit(solution)/shard_map/dot_general | solution.py:154
  158.7 2.9 %copy.91 = bf16[16,36,16,128]{3,0,1,2:T(8,128)(2,1)} copy(bf16[16,36,16,128]{3,2,1,0:T(8,128)(2,1)S(1)} %bitcast.122) | data formatting | bytes 4718592 | tf_op jit(solution)/shard_map/reshape;reshape | solution.py:39
  161.6 4.8 %all-to-all-start.2 = ((bf16[16,16,36,128]{3,1,2,0:T(8,128)(2,1)}), bf16[16,16,36,128]{3,1,2,0:T(8,128)(2,1)S(1)}, u32[]{:S(2)}, u32[]{:S(2)}) async-start(bf16[16,16,36,128]{3,1,2,0:T(8,128)(2,1)} %bitcast.121), calls=%async_computation.2 | async-start | bytes 4718592 | tf_op jit(solution)/shard_map/all_to_all | solution.py:44
  166.5 5.0 %all-gather.4.cloned.1.call-done = bf16[4096,256]{0,1:T(8,128)(2,1)} async-done(((bf16[256,256]{0,1:T(8,128)(2,1)}), bf16[4096,256]{0,1:T(8,128)(2,1)}) %all-gather.4.cloned.1.call-update) | async-done | bytes 2097168 | tf_op jit(solution)/shard_map/all_gather | solution.py:15
  171.4 2.1 fusion.82
  175.1 1.5 fusion.35
  177.3 48.7 %all-to-all-done.2 = bf16[16,16,36,128]{3,1,2,0:T(8,128)(2,1)S(1)} async-done(((bf16[16,16,36,128]{3,1,2,0:T(8,128)(2,1)}), bf16[16,16,36,128]{3,1,2,0:T(8,128)(2,1)S(1)}, u32[]{:S(2)}, u32[]{:S(2)}) %all-to-all-start.2) | async-done | bytes 2359328 | tf_op jit(solution)/shard_map/all_to_all | solution.py:44
  227.0 4.4 %all-to-all-start.3 = ((bf16[16,36,128]{2,1,0:T(8,128)(2,1)}), bf16[16,36,128]{2,1,0:T(8,128)(2,1)S(1)}, u32[]{:S(2)}, u32[]{:S(2)}) async-start(bf16[16,36,128]{2,1,0:T(8,128)(2,1)} %copy.69), calls=%async_computation.3 | async-start | bytes 327680 | tf_op jit(solution)/shard_map/all_to_all | solution.py:157
  233.0 2.3 convolution_convert_fusion.1
  235.3 11.1 %all-to-all-done.3 = bf16[16,36,128]{2,1,0:T(8,128)(2,1)S(1)} async-done(((bf16[16,36,128]{2,1,0:T(8,128)(2,1)}), bf16[16,36,128]{2,1,0:T(8,128)(2,1)S(1)}, u32[]{:S(2)}, u32[]{:S(2)}) %all-to-all-start.3) | async-done | bytes 147488 | tf_op jit(solution)/shard_map/all_to_all | solution.py:157
  246.4 1.4 gather_fusion.1
  (80 shorter events, 15.2 us)
Async XLA Ops:
  7.2 146.5 %copy-start = (bf16[1,128,2048]{2,1,0:T(8,128)(2,1)S(1)}, bf16[1,128,2048]{2,1,0:T(8,128)(2,1)}, u32[]{:S(2)}) copy-start(bf16[1,128,2048]{2,1,0:T(8,128)(2,1)} %param.27) | copy-start | bytes 1572868
  10.6 12.4 %copy-start.8 = (s32[384]{0:T(512)}, s32[384]{0:T(512)S(1)}, u32[]{:S(2)}) copy-start(s32[384]{0:T(512)S(1)} %fusion.75) | copy-start | bytes 4612
  25.8 59.0 %all-to-all-start = ((bf16[16,36,128]{2,1,0:T(8,128)(2,1)}), bf16[16,36,128]{2,1,0:T(8,128)(2,1)S(1)}, u32[]{:S(2)}, u32[]{:S(2)}) async-start(bf16[16,36,128]{2,1,0:T(8,128)(2,1)} %dynamic-slice_select_fusion), calls=%async_computation | async-start | bytes 327680 | tf_op jit(solution)/shard_map/all_to_all | solution.py:147
  86.7 9.0 %copy-start.5 = (bf16[256,128]{1,0:T(8,128)(2,1)S(1)}, bf16[256,128]{1,0:T(8,128)(2,1)}, u32[]{:S(2)}) copy-start(bf16[256,128]{1,0:T(8,128)(2,1)} %param.14) | copy-start | bytes 196612
  86.7 9.4 %copy-start.9 = (f32[128]{0:T(128)S(1)}, f32[128]{0:T(128)}, u32[]{:S(2)}) copy-start(f32[128]{0:T(128)} %param.18) | copy-start | bytes 1540
  86.7 9.5 %copy-start.10 = (f32[128]{0:T(128)S(1)}, f32[128]{0:T(128)}, u32[]{:S(2)}) copy-start(f32[128]{0:T(128)} %param.17) | copy-start | bytes 1540
  86.7 62.5 %all-to-all-start.1 = ((bf16[16,16,36,128]{3,1,2,0:T(8,128)(2,1)}), bf16[16,16,36,128]{3,1,2,0:T(8,128)(2,1)S(1)}, u32[]{:S(2)}, u32[]{:S(2)}) async-start(bf16[16,16,36,128]{3,1,2,0:T(8,128)(2,1)} %broadcast_in_dim.30), calls=%async_computation.1 | async-start | bytes 4718592 | tf_op jit(solution)/shard_map/all_to_all | solution.py:30
  94.5 76.9 %all-gather.4.cloned.1.call-start = ((), (), s32[]{:S(2)}) async-start(), calls=%async_computation.4 | async-start | bytes 2228224 | tf_op jit(solution)/shard_map/all_gather | solution.py:15
  149.2 2.9 %copy-start.11 = (bf16[1,2048,128]{2,1,0:T(8,128)(2,1)S(1)}, bf16[1,2048,128]{2,1,0:T(8,128)(2,1)}, u32[]{:S(2)}) copy-start(bf16[1,2048,128]{2,1,0:T(8,128)(2,1)} %param.25) | copy-start | bytes 1572868
  150.8 1.4 copy-start.1
  152.2 1.5 copy-start.3
  161.6 64.4 %all-to-all-start.2 = ((bf16[16,16,36,128]{3,1,2,0:T(8,128)(2,1)}), bf16[16,16,36,128]{3,1,2,0:T(8,128)(2,1)S(1)}, u32[]{:S(2)}, u32[]{:S(2)}) async-start(bf16[16,16,36,128]{3,1,2,0:T(8,128)(2,1)} %bitcast.121), calls=%async_computation.2 | async-start | bytes 4718592 | tf_op jit(solution)/shard_map/all_to_all | solution.py:44
  166.4 66.6 %all-gather.6.cloned.1.call-start = ((), (), s32[]{:S(2)}) async-start(), calls=%async_computation.5 | async-start | bytes 1114112 | tf_op jit(solution)/shard_map/all_gather | solution.py:124
  173.5 1.6 copy-start.2
  175.1 1.5 copy-start.6
  176.6 56.4 %copy-start.4 = (bf16[2048,128]{1,0:T(8,128)(2,1)S(1)}, bf16[2048,128]{1,0:T(8,128)(2,1)}, u32[]{:S(2)}) copy-start(bf16[2048,128]{1,0:T(8,128)(2,1)} %param.19) | copy-start | bytes 1572868
  176.7 0.6 copy-start.7
  227.0 19.4 %all-to-all-start.3 = ((bf16[16,36,128]{2,1,0:T(8,128)(2,1)}), bf16[16,36,128]{2,1,0:T(8,128)(2,1)S(1)}, u32[]{:S(2)}, u32[]{:S(2)}) async-start(bf16[16,36,128]{2,1,0:T(8,128)(2,1)} %copy.69), calls=%async_computation.3 | async-start | bytes 327680 | tf_op jit(solution)/shard_map/all_to_all | solution.py:157
Sparse Core Ops, SparseCore 0:
  97.6 73.7 all-gather.3
  176.8 50.3 all-gather.5
where the time goes:
time: 256 us
  waiting for transfers between devices  132 us (52%)
  starting transfers between devices  60.9 us (24%)
  local copies, waits for them, and re-layouts  26.2 us (10%)
  between operations  14.4 us (6%)
  matrix products  11.6 us (5%)
  other arithmetic  10.6 us (4%)
    all_to_all x1, waiting for transfers between devices, copy_for_each(): return lax.all_to_all(copies, axis, split_axis=0, concat_axis=0, tiled=True)  51.7 us
    all_to_all x1, waiting for transfers between devices, sent_and_summed(): lax.all_to_all(blocks, axis, split_axis=0, concat_axis=0, tiled=True)  48.7 us
    all_to_all x1, starting transfers between devices, per_device(): lax.all_to_all(mine, 'ep', split_axis=0, concat_axis=0, tiled=True)  43.7 us
    all_to_all x1, waiting for transfers between devices, per_device(): lax.all_to_all(mine, 'ep', split_axis=0, concat_axis=0, tiled=True)  15.3 us
    all_to_all x1, waiting for transfers between devices, per_device(): back = lax.all_to_all(summed, 'ep', split_axis=0, concat_axis=0, tiled=True)  11.1 us
    all_to_all x1, starting transfers between devices, copy_for_each(): return lax.all_to_all(copies, axis, split_axis=0, concat_axis=0, tiled=True)  7.76 us
    gather x2, local copies, waits for them, and re-layouts, per_device(): normed[source]  6.61 us
  transfers between devices with their start and end apart: 6, of which 5 were waited for; matrix products, arithmetic and copies ran while one was open for 9% of the time, Pallas kernels for 0%

commit v1 on v0

v1 whole, which is shorter than its diff:
```python
import functools

import jax
import jax.numpy as jnp
from jax import lax
from jax.experimental import pallas as pl
from jax.experimental.pallas import tpu as pltpu
from jax.sharding import PartitionSpec as P

HEADS = 16
KV_HEADS = 4
HEAD_DIM = 128
GRID_W = 64
TOPK = 2
W = 128
PAD = 48
MESH = pl.DeviceIdType.MESH
f32 = jnp.float32
bf16 = jnp.bfloat16


def remote(src, dst, ss, rs, dev):
    return pltpu.make_async_remote_copy(
        src_ref=src, dst_ref=dst, send_sem=ss, recv_sem=rs, device_id=dev, device_id_type=MESH
    )


def near_first(n):
    order = [0]
    for i in range(1, n // 2 + 1):
        order += [i] if 2 * i == n else [i, n - i]
    return order


def moe_kernel(
    nz,
    nt,
    rows_hbm,
    routes_ref,
    ggate_ref,
    logits_ref,
    gain_ref,
    wg_hbm,
    wu_hbm,
    wd_hbm,
    out_ref,
    rows_v,
    w13,
    wdp,
    sendb,
    recvb,
    xall,
    pairs,
    psend,
    precv,
    rs_send,
    rs_recv,
    ret_send,
    ret_recv,
    smat,
    lsem,
    wsem,
    disp_s,
    disp_r,
    ag_s,
    ag_r,
    dd_s,
    dd_r,
    pr_s,
    pr_r,
    rss_s,
    rss_r,
    ret_s,
    ret_r,
):
    count, width = rows_v.shape
    nx = nt // 2
    half = nx // 2
    cap = 3 * count // nz
    nchunk = nz // 4
    R = 4 * cap
    RP = 4 * PAD
    up_rows = 80
    order = near_first(nz)
    pos = {d: p for p, d in enumerate(order)}
    color = nx * W

    z = lax.axis_index("ep")
    t = lax.axis_index("tp")
    x = t // 2
    c = t % 2
    right = ((x + 1) % nx) * 2 + c
    left = ((x + nx - 1) % nx) * 2 + c
    other = x * 2 + (1 - c)

    def lane(i):
        return pl.ds(pl.multiple_of(i * W, W), W)

    barrier = pltpu.get_barrier_semaphore()
    for d in order[1:][::-1]:
        pl.semaphore_signal(barrier, inc=1, device_id={"ep": (z + d) % nz}, device_id_type=MESH)
    for who in (right, left, other):
        pl.semaphore_signal(barrier, inc=1, device_id={"tp": who}, device_id_type=MESH)

    load_rows = pltpu.make_async_copy(rows_hbm, rows_v, lsem.at[0])
    load_g = pltpu.make_async_copy(wg_hbm, w13.at[:, 0:W], lsem.at[1])
    load_u = pltpu.make_async_copy(wu_hbm, w13.at[:, W : 2 * W], lsem.at[2])
    load_rows.start()
    load_g.start()
    load_u.start()
    load_d = []
    for k in range(2):
        for dx in range(nx):
            core = c if k == 0 else 1 - c
            col = ((x + dx) % nx) * 2 + core
            at = k * color + dx * W
            load_d.append(
                pltpu.make_async_copy(
                    wd_hbm.at[:, lane(col)], wdp.at[:, at : at + W], wsem.at[k * nx + dx]
                )
            )
            load_d[-1].start()

    e_lane = lax.broadcasted_iota(jnp.int32, (count, W), 1)
    r0 = routes_ref[:, 0:1]
    r1 = routes_ref[:, 1:2]
    named = jnp.where((r0 == e_lane) | (r1 == e_lane), 1.0, 0.0).astype(bf16)
    named0 = jnp.where(r0 == e_lane, 1.0, 0.0).astype(bf16)
    before = jnp.where(
        lax.broadcasted_iota(jnp.int32, (count, count), 1)
        < lax.broadcasted_iota(jnp.int32, (count, count), 0),
        1.0,
        0.0,
    ).astype(bf16)
    rank = jnp.dot(before, named, preferred_element_type=f32).astype(bf16)
    col_e = lax.broadcasted_iota(jnp.int32, (W, nz * PAD), 1)
    row_e = lax.broadcasted_iota(jnp.int32, (W, nz * PAD), 0)
    lo = row_e * PAD
    spread = jnp.where((col_e >= lo) & (col_e < lo + PAD), 1.0, 0.0).astype(bf16)
    slot_of = (
        lax.broadcasted_iota(jnp.int32, (1, nz * PAD), 1) % PAD
    ).astype(f32)
    named_x = jnp.dot(named, spread, preferred_element_type=f32)
    named0_x = jnp.dot(named0, spread, preferred_element_type=f32)
    rank_x = jnp.dot(rank, spread, preferred_element_type=f32)
    hit = (named_x > 0.5) & (jnp.abs(rank_x - slot_of) < 0.5)
    hit0 = hit & (named0_x > 0.5)
    s_all = jnp.where(hit, 1.0, 0.0)
    s_0 = jnp.where(hit0, 1.0, 0.0)
    smat[0] = s_0.astype(bf16)
    smat[1] = (s_all - s_0).astype(bf16)

    load_rows.wait()
    wide = rows_v[...].astype(f32)
    inv = lax.rsqrt(jnp.mean(wide * wide, axis=-1, keepdims=True) + 1e-06)
    mine = rows_v[:, lane(t)].astype(f32) * inv * gain_ref[:, lane(t)]
    sendb[...] = lax.dot_general(
        s_all.astype(bf16), mine.astype(bf16), (((0,), (0,)), ((), ())), preferred_element_type=f32
    ).astype(bf16)

    pl.semaphore_wait(barrier, nz - 1 + 3)

    def block(i):
        return pl.ds(pl.multiple_of(i * PAD, PAD), PAD)

    def disp(d):
        to = (z + d) % nz
        p = pos[(nz - d) % nz]
        return remote(
            sendb.at[block(to)],
            recvb.at[p * PAD : (p + 1) * PAD],
            disp_s.at[d],
            disp_r.at[p],
            {"ep": to},
        )

    def disp_in(p):
        d = (nz - order[p]) % nz
        return disp(d)

    for d in order[1:]:
        disp(d).start()
    recvb[0:PAD] = sendb[block(z)]

    pr = lax.broadcasted_iota(jnp.int32, (R, RP), 0)
    pc = lax.broadcasted_iota(jnp.int32, (R, RP), 1)
    pack = jnp.where((pr // cap == pc // PAD) & (pr % cap == pc % PAD), 1.0, 0.0).astype(bf16)

    def at_rows(k):
        return pl.ds(pl.multiple_of(k * R, R), R)

    def ag(k, side, s):
        xo = (x + nx - (s - 1)) % nx if side == 0 else (x + s - 1) % nx
        cols = lane(xo * 2 + c)
        if s < half:
            part = at_rows(k)
        elif side == 0:
            part = pl.ds(pl.multiple_of(k * R, 16), up_rows)
        else:
            part = pl.ds(pl.multiple_of(k * R + up_rows, 16), R - up_rows)
        view = xall.at[part, cols]
        to = right if side == 0 else left
        return remote(view, view, ag_s.at[k, side, s - 1], ag_r.at[k, side, s - 1], {"tp": to})

    def ag_in(k, side, s):
        return ag(k, side, s)

    def dd(k, j, mine_side):
        core = c if mine_side else 1 - c
        rows = at_rows(k)
        if j == 0:
            xo = x
        elif j <= half - 1:
            xo = (x + nx - j) % nx
        elif j <= 2 * half - 2:
            xo = (x + j - (half - 1)) % nx
        else:
            xo = (x + half) % nx
            if j == 2 * half - 1:
                rows = pl.ds(pl.multiple_of(k * R, 16), up_rows)
            else:
                rows = pl.ds(pl.multiple_of(k * R + up_rows, 16), R - up_rows)
        view = xall.at[rows, lane(xo * 2 + core)]
        return remote(view, view, dd_s.at[k, j], dd_r.at[k, j], {"tp": other})

    ndd = 2 * half + 1

    for k in range(nchunk):
        for p in range(4 * k, 4 * k + 4):
            if p:
                disp_in(p).wait_recv()
        packed = jnp.dot(pack, recvb[k * RP : (k + 1) * RP], preferred_element_type=f32)
        xall[k * R : (k + 1) * R, lane(t)] = packed.astype(bf16)
        ag(k, 0, 1).start()
        ag(k, 1, 1).start()
        dd(k, 0, True).start()

    for s in range(1, half + 1):

        def hop(k, carry, s=s):
            for side in range(2):
                ag_in(k, side, s).wait_recv()
                if s < half:
                    ag(k, side, s + 1).start()
                    dd(k, s if side == 0 else half - 1 + s, True).start()
                else:
                    dd(k, 2 * half - 1 + side, True).start()
            return carry

        lax.fori_loop(0, nchunk, hop, 0)

    load_g.wait()
    load_u.wait()
    for cp in load_d:
        cp.wait()

    def pair(k):
        return remote(psend.at[k], precv.at[k], pr_s.at[k], pr_r.at[k], {"tp": other})

    def ffn(k, carry):
        for j in range(ndd):
            dd(k, j, False).wait_recv()
        xk = xall[at_rows(k), :]
        h = jnp.dot(xk, w13[...], preferred_element_type=f32)
        g = h[:, 0:W]
        hidden = (g * jax.nn.sigmoid(g) * h[:, W : 2 * W]).astype(bf16)
        part = jnp.dot(hidden, wdp[...], preferred_element_type=f32).astype(bf16)
        psend[k] = part[:, color:]
        pairs[k] = part[:, :color].astype(f32)
        pair(k).start()
        return carry

    lax.fori_loop(0, nchunk, ffn, 0)

    def part_rows(side, s):
        if s > 1:
            return 0, R
        return (0, up_rows) if side == 0 else (up_rows, R)

    def rs(k, side, s):
        a, b = part_rows(side, s)
        to = right if side == 0 else left
        return remote(
            rs_send.at[k, side, s - 1, a:b],
            rs_recv.at[k, side, s - 1, a:b],
            rss_s.at[k, side, s - 1],
            rss_r.at[k, side, s - 1],
            {"tp": to},
        )

    def target(side, s):
        far = half + 1 - s
        return far if side == 0 else nx - far

    def rs_first(k, carry):
        pair(k).wait_recv()
        pairs[k] = pairs[k] + precv[k].astype(f32)
        for side in range(2):
            a, b = part_rows(side, 1)
            at = target(side, 1) * W
            rs_send[k, side, 0, a:b] = pairs[k, a:b, at : at + W].astype(bf16)
            rs(k, side, 1).start()
        return carry

    lax.fori_loop(0, nchunk, rs_first, 0)

    for s in range(2, half + 1):

        def rs_hop(k, carry, s=s):
            for side in range(2):
                rs(k, side, s - 1).wait_recv()
                at = target(side, s) * W
                a, b = part_rows(side, s - 1)
                rs_send[k, side, s - 1, a:b] = (
                    pairs[k, a:b, at : at + W] + rs_recv[k, side, s - 2, a:b].astype(f32)
                ).astype(bf16)
                if a > 0:
                    rs_send[k, side, s - 1, 0:a] = pairs[k, 0:a, at : at + W].astype(bf16)
                if b < R:
                    rs_send[k, side, s - 1, b:R] = pairs[k, b:R, at : at + W].astype(bf16)
                rs(k, side, s).start()
            return carry

        lax.fori_loop(0, nchunk, rs_hop, 0)

    ur = lax.broadcasted_iota(jnp.int32, (RP, R), 0)
    uc = lax.broadcasted_iota(jnp.int32, (RP, R), 1)
    unpack = jnp.where((uc // cap == ur // PAD) & (uc % cap == ur % PAD), 1.0, 0.0).astype(bf16)

    def ret(d):
        p = pos[d]
        return remote(
            ret_send.at[p * PAD : (p + 1) * PAD],
            ret_recv.at[block(z)],
            ret_s.at[d],
            ret_r.at[(nz - d) % nz],
            {"ep": (z + d) % nz},
        )

    def ret_in(d):
        view = ret_recv.at[block((z + d) % nz)]
        return remote(view, view, ret_s.at[d], ret_r.at[d], {"ep": (z + d) % nz})

    for k in range(nchunk):
        for side in range(2):
            rs(k, side, half).wait_recv()
            a, b = part_rows(side, half)
            pairs[k, a:b, 0:W] = pairs[k, a:b, 0:W] + rs_recv[k, side, half - 1, a:b].astype(f32)
        y = pairs[k, :, 0:W].astype(bf16)
        ret_send[k * RP : (k + 1) * RP] = jnp.dot(unpack, y, preferred_element_type=f32).astype(
            bf16
        )
        for p in range(4 * k, 4 * k + 4):
            if p:
                ret(order[p]).start()
    ret_recv[block(z)] = ret_send[0:PAD]

    logits = logits_ref[...]
    top = jnp.max(logits, axis=-1, keepdims=True)
    ex = jnp.exp(logits - top)
    soft = ex / jnp.sum(ex, axis=-1, keepdims=True)
    eye = lax.broadcasted_iota(jnp.int32, (count, count), 0) == lax.broadcasted_iota(
        jnp.int32, (count, count), 1
    )
    gg = jnp.sum(jnp.where(eye, ggate_ref[...], 0.0), axis=1, keepdims=True)
    weights = gg * soft

    for d in order[1:]:
        ret_in(d).wait_recv()
    table = ret_recv[...]
    p0 = jnp.dot(smat[0], table, preferred_element_type=f32)
    p1 = jnp.dot(smat[1], table, preferred_element_type=f32)
    out_ref[...] = (weights[:, 0:1] * p0 + weights[:, 1:2] * p1).astype(bf16)

    for d in order[1:]:
        disp(d).wait_send()
        ret(d).wait_send()

    def drain(k, carry):
        for side in range(2):
            for s in range(1, half + 1):
                ag(k, side, s).wait_send()
                rs(k, side, s).wait_send()
        for j in range(ndd):
            dd(k, j, True).wait_send()
        pair(k).wait_send()
        return carry

    lax.fori_loop(0, nchunk, drain, 0)


def moe(mesh, rows, routes, ggate, logits, gain, wg, wu, wd):
    nz, nt = mesh.shape["ep"], mesh.shape["tp"]
    count, width = rows.shape
    nx = nt // 2
    half = nx // 2
    cap = 3 * count // nz
    k = nz // 4
    R = 4 * cap
    color = nx * W
    dma = pltpu.SemaphoreType.DMA
    vmem = pl.BlockSpec(memory_space=pltpu.VMEM)
    hbm = pl.BlockSpec(memory_space=pl.ANY)
    return pl.pallas_call(
        functools.partial(moe_kernel, nz, nt),
        out_shape=jax.ShapeDtypeStruct((count, W), bf16),
        in_specs=[hbm, vmem, vmem, vmem, vmem, hbm, hbm, hbm],
        out_specs=vmem,
        scratch_shapes=[
            pltpu.VMEM((count, width), bf16),
            pltpu.VMEM((width, 2 * W), bf16),
            pltpu.VMEM((W, width), bf16),
            pltpu.VMEM((nz * PAD, W), bf16),
            pltpu.VMEM((nz * PAD, W), bf16),
            pltpu.VMEM((k * R, width), bf16),
            pltpu.VMEM((k, R, color), f32),
            pltpu.VMEM((k, R, color), bf16),
            pltpu.VMEM((k, R, color), bf16),
            pltpu.VMEM((k, 2, half, R, W), bf16),
            pltpu.VMEM((k, 2, half, R, W), bf16),
            pltpu.VMEM((nz * PAD, W), bf16),
            pltpu.VMEM((nz * PAD, W), bf16),
            pltpu.VMEM((2, count, nz * PAD), bf16),
            dma((3,)),
            dma((2 * nx,)),
            dma((nz,)),
            dma((nz,)),
            dma((k, 2, half)),
            dma((k, 2, half)),
            dma((k, 2 * half + 1)),
            dma((k, 2 * half + 1)),
            dma((k,)),
            dma((k,)),
            dma((k, 2, half)),
            dma((k, 2, half)),
            dma((nz,)),
            dma((nz,)),
        ],
        compiler_params=pltpu.CompilerParams(collective_id=0, has_side_effects=True),
        name="moe",
    )(rows, routes, ggate, logits, gain, wg, wu, wd)


def head_norm(x, gain):
    wide = x.astype(jnp.float32)
    return wide * lax.rsqrt(jnp.mean(wide * wide, axis=-1, keepdims=True) + 1e-06) * gain


def rotate(x, first):
    count = x.shape[0]
    pos = first + jnp.arange(count, dtype=jnp.int32)
    row = (pos // GRID_W).astype(jnp.float32)
    col = (pos % GRID_W).astype(jnp.float32)
    nfreq = HEAD_DIM // 4
    inverse = 10000.0 ** (-jnp.arange(nfreq, dtype=jnp.float32) / nfreq)
    angle = jnp.concatenate(
        [
            row[:, None] * inverse,
            row[:, None] * inverse,
            col[:, None] * inverse,
            col[:, None] * inverse,
        ],
        axis=1,
    )
    parts = x.reshape(x.shape[:-1] + (2, 2, nfreq))
    turned = jnp.stack([-parts[..., 1, :], parts[..., 0, :]], axis=-2).reshape(x.shape)
    return x * jnp.cos(angle)[:, None, :] + turned * jnp.sin(angle)[:, None, :]


def attention(queries, keys, values, q_gain, k_gain, w_out):
    rows = queries.shape[0]
    heads_dev = queries.shape[1] // HEAD_DIM
    group = HEADS // KV_HEADS
    kv_dev = max(1, heads_dev // group)
    per_kv = heads_dev // kv_dev
    first_kv = lax.axis_index("tp") * heads_dev // group
    first_row = lax.axis_index("ep") * rows
    k_mine = lax.dynamic_slice_in_dim(keys, first_kv * HEAD_DIM, kv_dev * HEAD_DIM, 1)
    v_mine = lax.dynamic_slice_in_dim(values, first_kv * HEAD_DIM, kv_dev * HEAD_DIM, 1)
    k_rot = rotate(head_norm(k_mine.reshape(rows, kv_dev, HEAD_DIM), k_gain), first_row)
    k_rot = k_rot.astype(jnp.bfloat16).reshape(rows, kv_dev * HEAD_DIM)
    q_rot = rotate(head_norm(queries.reshape(rows, heads_dev, HEAD_DIM), q_gain), first_row)
    q_rot = q_rot.astype(jnp.bfloat16).reshape(rows, kv_dev, per_kv, HEAD_DIM)
    scale = HEAD_DIM ** (-0.5)
    both = lax.all_gather(jnp.concatenate([k_rot, v_mine], 1), "ep", axis=0, tiled=True)
    k_piece, v_piece = both[:, : kv_dev * HEAD_DIM], both[:, kv_dev * HEAD_DIM :]
    count = k_piece.shape[0]
    key_rows = k_piece.reshape(count, kv_dev, HEAD_DIM)
    value_rows = v_piece.reshape(count, kv_dev, HEAD_DIM)
    scores = (
        jnp.einsum("qkgd,nkd->qkgn", q_rot, key_rows, preferred_element_type=jnp.float32) * scale
    )
    top = jnp.max(scores, axis=-1)
    expo = jnp.exp(scores - top[..., None])
    total = jnp.sum(expo, axis=-1)
    acc = jnp.einsum(
        "qkgn,nkd->qkgd", expo.astype(jnp.bfloat16), value_rows, preferred_element_type=jnp.float32
    )
    mixed = (acc / total[..., None]).astype(jnp.bfloat16).reshape(rows, heads_dev * HEAD_DIM)
    return jnp.dot(
        lax.all_gather(mixed, "tp", axis=1, tiled=True), w_out, preferred_element_type=jnp.float32
    ).astype(jnp.bfloat16)


def solution(mesh):
    def per_device(
        queries, keys, values, q_gain, k_gain, w_out, moe_rows, routes,
        group_gate, expert_logits, moe_gain, w_gate, w_up, w_down,
    ):
        attn_out = attention(queries, keys, values, q_gain, k_gain, w_out)
        moe_out = moe(
            mesh,
            moe_rows,
            routes,
            group_gate.reshape(1, -1),
            expert_logits,
            moe_gain.reshape(1, -1),
            w_gate[0],
            w_up[0],
            w_down[0],
        )
        return attn_out, moe_out

    placed = (
        P(("grp", "ep"), "tp"),
        P(("grp", "ep"), None),
        P(("grp", "ep"), None),
        P(),
        P(),
        P(None, "tp"),
        P(("grp", "ep"), None),
        P(("grp", "ep"), None),
        P(("grp", "ep")),
        P(("grp", "ep"), None),
        P(),
        P("ep", None, "tp"),
        P("ep", None, "tp"),
        P("ep", "tp", None),
    )
    return jax.shard_map(
        per_device,
        mesh=mesh,
        in_specs=placed,
        out_specs=(P(("grp", "ep"), "tp"), P(("grp", "ep"), "tp")),
        check_vma=False,
    )
```

time: 256 us -> 209 us (0.82)
  Pallas kernels: 0 us -> 65 us
  starting transfers between devices: 60.9 us -> 0.13 us
  local copies, waits for them, and re-layouts: 26.2 us -> 5.05 us
  waiting for transfers between devices: 132 us -> 114 us
  other arithmetic: 10.6 us -> 4.19 us
  matrix products: 11.6 us -> 6.05 us
    all_to_all x4 -> x0, waiting for transfers between devices: 127 us -> none  [the longest x1 51.7 us: copy_for_each(): return lax.all_to_all(copies, axis, split_axis=0, concat_axis=0, tiled=True)]
    all_gather x2, waiting for transfers between devices: 4.97 us -> 114 us  [the longest x1 114 us: attention(): lax.all_gather(jnp.concatenate([k_rot, v_mine], 1), 'ep', axis=0, tiled=T...]
    pallas_call x0 -> x1, Pallas kernels: none -> 65 us  [moe(): pl.pallas_call(functools.partial(moe_kernel, nz, nt), out_shape=jax.Shape...]
    all_to_all x4 -> x0, starting transfers between devices: 60.6 us -> none  [the longest x1 43.7 us: per_device(): lax.all_to_all(mine, 'ep', split_axis=0, concat_axis=0, tiled=True)]
    gather x3 -> x0, local copies, waits for them, and re-layouts: 8.05 us -> none  [the longest x2 6.61 us: per_device(): normed[source]]
    dot_general x5 -> x3, matrix products: 11.6 us -> 6.05 us  [the longest x1 2.33 us: attention(): jnp.dot(lax.all_gather(mixed, 'tp', axis=1, tiled=True), w_out, preferred...]
    scatter x2 -> x0, local copies, waits for them, and re-layouts: 4.89 us -> none  [the longest x1 2.92 us: per_device(): source = jnp.zeros((peers * capacity,), jnp.int32).at[slots].set(owner)]
    reduce_sum x6 -> x1, other arithmetic: 3.93 us -> 0.63 us  [attention(): total = jnp.sum(expo, axis=-1)]
  transfers between devices with their start and end apart: 6 -> 2, of which waited for: 5 -> 1; matrix products, arithmetic and copies ran while one was open for 9% -> 1% of each run, Pallas kernels for 0% -> 31%
where the time goes in v1:
time: 209 us
  waiting for transfers between devices  114 us (55%)
  Pallas kernels  65 us (31%)
  between operations  14.2 us (7%)
  matrix products  6.05 us (3%)
  local copies, waits for them, and re-layouts  5.05 us (2%)
  other arithmetic  4.19 us (2%)
    all_gather x1, waiting for transfers between devices, attention(): lax.all_gather(jnp.concatenate([k_rot, v_mine], 1), 'ep', axis=0, tiled=T...  114 us
    pallas_call x1, Pallas kernels, moe(): pl.pallas_call(functools.partial(moe_kernel, nz, nt), out_shape=jax.Shape...  65 us
  transfers between devices with their start and end apart: 2, of which 1 were waited for; matrix products, arithmetic and copies ran while one was open for 1% of the time, Pallas kernels for 31%

profile of v1, /device:TPU:80, one launch (start us, length us, event | category | flops | bytes accessed | tf_op | source)
XLA Modules:
  0.0 208.6 jit_solution(5380383716275202840)
XLA Ops:
  7.2 0.0 copy-start
  7.2 0.1 all-gather.4.cloned.1.call-start
  7.3 0.9 constant_dynamic-slice_fusion
  8.2 0.1 copy.23
  8.4 0.7 fusion.23
  9.2 0.9 copy.20
  10.1 0.7 fusion.25
  10.9 0.1 copy.24
  11.1 0.1 broadcast_multiply_fusion.1
  11.2 1.2 fusion.29
  12.4 0.7 pad_maximum_fusion.2
  13.0 0.1 all-gather.4.cloned.1.call-update
  13.1 0.1 all-gather.6.cloned.1.call-start
  13.2 113.8 %all-gather.4.cloned.1.call-done = bf16[4096,256]{0,1:T(8,128)(2,1)} async-done(((bf16[256,256]{0,1:T(8,128)(2,1)}), bf16[4096,256]{0,1:T(8,128)(2,1)}) %all-gather.4.cloned.1.call-update) | async-done | bytes 2097168 | tf_op jit(solution)/shard_map/all_gather | solution.py:485
  127.0 2.2 %fusion.35 = (f32[256]{0:T(256)S(1)}, f32[4096,256]{1,0:T(8,128)S(1)}) fusion(bf16[256,128]{0,1:T(8,128)(2,1)S(1)} %get-tuple-element.7, bf16[4096,256]{0,1:T(8,128)(2,1)} %all-gather.4.cloned.1.call-done), kind=kOutput, calls=%fused_computation.55 | convolution fusion | flops 270532352 | bytes 5309440 | tf_op jit(solution)/shard_map/qkgd,nkd->qkgn/dot_general | solution.py:491
  129.2 0.6 fusion.1
  129.9 1.5 fusion.16
  131.4 0.1 all-gather.6.cloned.1.call-update
  131.4 0.8 copy.21.routes_ref
  132.2 0.8 copy.22.logits_ref
  133.0 65.0 %moe.1 = bf16[192,128]{1,0:T(8,128)(2,1)} custom-call(bf16[192,2048]{1,0:T(8,128)(2,1)} %rows_hbm.1, s32[192,2]{1,0:T(8,128)} %copy.21.routes_ref, f32[1,192]{1,0:T(1,128)} %bitcast.72, f32[192,2]{1,0:T(8,128)} %copy.22.logits_ref, f32[1,2048]{1,0:T(1,128)} %bitcast.71, bf16[2048,128]{1,0:T(8,128)(2,1)} %bitcast.66, bf16[2048,128]{1,0:T(8,128)(2,1)} %bitcast.67, ...), custom_call_target="tpu_custom_call" | custom-call | tf_op jit(solution)/shard_map/moe/pallas_call | solution.py:404
  198.0 0.0 all-gather.6.cloned.1.call-done
  198.0 2.3 %convolution_convert_fusion = bf16[256,128]{1,0:T(8,128)(2,1)} fusion(bf16[2048,128]{1,0:T(8,128)(2,1)S(1)} %copy-done, bf16[256,1,1,2048]{0,3,2,1:T(8,128)(2,1)} %all-gather.6.cloned.1.call-done), kind=kOutput, calls=%fused_computation.9 | convolution fusion | flops 134250496 | bytes 1638400 | tf_op jit(solution)/shard_map/dot_general | solution.py:500
  200.3 1.4 copy.26
  (17 shorter events, 0.2 us)
Async XLA Ops:
  7.2 190.8 %copy-start = (bf16[2048,128]{1,0:T(8,128)(2,1)S(1)}, bf16[2048,128]{1,0:T(8,128)(2,1)}, u32[]{:S(2)}) copy-start(bf16[2048,128]{1,0:T(8,128)(2,1)} %param.19) | copy-start | bytes 1572868
  7.2 119.8 %all-gather.4.cloned.1.call-start = ((), (), s32[]{:S(2)}) async-start(), calls=%async_computation | async-start | bytes 2228224 | tf_op jit(solution)/shard_map/all_gather | solution.py:485
  13.1 184.9 %all-gather.6.cloned.1.call-start = ((), (), s32[]{:S(2)}) async-start(), calls=%async_computation.1 | async-start | bytes 1114112 | tf_op jit(solution)/shard_map/all_gather | solution.py:501
  127.0 2.9 %copy-start.1 = (bf16[4096,256]{0,1:T(8,128)(2,1)S(1)}, bf16[4096,256]{0,1:T(8,128)(2,1)}, u32[]{:S(2)}) copy-start(bf16[4096,256]{0,1:T(8,128)(2,1)} %all-gather.4.cloned.1.call-done) | copy-start | bytes 6291460
  129.2 2.2 %copy-start.2 = (s32[192,2]{0,1:T(2,128)S(1)}, s32[192,2]{0,1:T(2,128)}, u32[]{:S(2)}) copy-start(s32[192,2]{0,1:T(2,128)} %param.21) | copy-start | bytes 4612
  129.2 3.0 %copy-start.3 = (f32[192,2]{0,1:T(2,128)S(1)}, f32[192,2]{0,1:T(2,128)}, u32[]{:S(2)}) copy-start(f32[192,2]{0,1:T(2,128)} %param.23) | copy-start | bytes 4612
Sparse Core Ops, SparseCore 0:
  13.2 113.7 all-gather.3
  131.5 40.1 all-gather.5

commit v2 on v0

v2 whole, which is shorter than its diff:
```python
import functools

import jax
import jax.numpy as jnp
from jax import lax
from jax.experimental import pallas as pl
from jax.experimental.pallas import tpu as pltpu
from jax.sharding import PartitionSpec as P

HEADS = 16
KV_HEADS = 4
HEAD_DIM = 128
GRID_W = 64
TOPK = 2
GROUP = HEADS // KV_HEADS
W = 128
PAD = 48
MESH = pl.DeviceIdType.MESH
f32 = jnp.float32
bf16 = jnp.bfloat16


def remote(src, dst, ss, rs, dev):
    return pltpu.make_async_remote_copy(
        src_ref=src, dst_ref=dst, send_sem=ss, recv_sem=rs, device_id=dev, device_id_type=MESH
    )


def near_first(n):
    order = [0]
    for i in range(1, n // 2 + 1):
        order += [i] if 2 * i == n else [i, n - i]
    return order


SCRATCH = (
    "queries_v",
    "k_raw",
    "kvb",
    "qs",
    "qgain_v",
    "kgain_v",
    "wout_v",
    "o_own",
    "lse_own",
    "po_send",
    "po_recv",
    "ls_send",
    "ls_recv",
    "heads",
    "rows_v",
    "routes_v",
    "ggate_v",
    "logits_v",
    "gain_v",
    "w13",
    "wdp",
    "sendb",
    "recvb",
    "xall",
    "pairs",
    "psend",
    "precv",
    "rs_send",
    "rs_recv",
    "ret_send",
    "ret_recv",
    "sslot",
    "smat",
    "wcol",
    "lsem",
    "wsem",
    "disp_s",
    "disp_r",
    "ag_s",
    "ag_r",
    "dd_s",
    "dd_r",
    "pr_s",
    "pr_r",
    "rss_s",
    "rss_r",
    "ret_s",
    "ret_r",
    "q_s",
    "q_r",
    "kva_s",
    "kva_r",
    "kvb_s",
    "kvb_r",
    "po_s",
    "po_r",
    "ls_s",
    "ls_r",
    "oag_s",
    "oag_r",
    "odd_s",
    "odd_r",
    "in_sem",
    "pack",
    "unpack",
)


def fused_kernel(nz, nt, *refs):
    (q_hbm, keys_hbm, values_hbm, qgain_hbm, kgain_hbm, wout_hbm, rows_hbm, routes_hbm, ggate_hbm, logits_hbm, gain_hbm, wg_hbm, wu_hbm, wd_hbm, attn_ref, out_ref) = refs[:16]
    s_ = dict(zip(SCRATCH, refs[16:], strict=True))
    queries_v, k_raw, kvb, qs, qgain_v, kgain_v, wout_v = (s_[n] for n in SCRATCH[:7])
    o_own, lse_own, po_send, po_recv, ls_send, ls_recv, heads = (s_[n] for n in SCRATCH[7:14])
    rows_v, routes_v, ggate_v, logits_v, gain_v, w13, wdp = (s_[n] for n in SCRATCH[14:21])
    sendb, recvb, xall, pairs, psend, precv, rs_send, rs_recv = (s_[n] for n in SCRATCH[21:29])
    ret_send, ret_recv, sslot, smat, wcol = (s_[n] for n in SCRATCH[29:34])
    lsem, wsem, disp_s, disp_r, ag_s, ag_r, dd_s, dd_r = (s_[n] for n in SCRATCH[34:42])
    pr_s, pr_r, rss_s, rss_r, ret_s, ret_r = (s_[n] for n in SCRATCH[42:48])
    q_s, q_r, kva_s, kva_r, kvb_s, kvb_r, po_s, po_r, ls_s, ls_r = (s_[n] for n in SCRATCH[48:58])
    oag_s, oag_r, odd_s, odd_r, in_sem, pack, unpack = (s_[n] for n in SCRATCH[58:65])

    count, width = rows_v.shape
    nx = nt // 2
    half = nx // 2
    cap = 3 * count // nz
    nchunk = nz // 4
    R = 4 * cap
    RP = 4 * PAD
    up_rows = 80
    order = near_first(nz)
    color = nx * W
    qrows = queries_v.shape[0]
    kq = qrows // GROUP
    nset = nz // 4
    setrows = nset * kq

    z = lax.axis_index("ep")
    t = lax.axis_index("tp")
    x = t // 2
    c = t % 2
    right = ((x + 1) % nx) * 2 + c
    left = ((x + nx - 1) % nx) * 2 + c
    other = x * 2 + (1 - c)
    xpair = x + 1 - 2 * (x % 2)
    mates = (None, other, xpair * 2 + c, xpair * 2 + 1 - c)
    quarter = t % GROUP
    kvh = t // GROUP

    def lane(i):
        return pl.ds(pl.multiple_of(i * W, W), W)

    with jax.named_scope("signal"):
        barrier = pltpu.get_barrier_semaphore()

        def greet(j, carry):
            @pl.when(j > z)
            def _():
                pl.semaphore_signal(barrier, inc=1, device_id={"ep": j}, device_id_type=MESH)

            return carry

        lax.fori_loop(0, nz, greet, 0)
        for who in (right, left, other, mates[2], mates[3]):
            pl.semaphore_signal(barrier, inc=1, device_id={"tp": who}, device_id_type=MESH)

        local = {}

        def fetch(name, src, dst):
            local[name] = pltpu.make_async_copy(src, dst, lsem.at[len(local)])
            local[name].start()

        fetch("routes", routes_hbm, routes_v)
        fetch("rows", rows_hbm, rows_v)
        fetch("gain", gain_hbm, gain_v)
        fetch("q", q_hbm, queries_v)
        fetch("k", keys_hbm.at[pl.ds(pl.multiple_of(quarter * kq, kq), kq), lane(kvh)], k_raw)
        fetch(
            "v",
            values_hbm.at[pl.ds(pl.multiple_of(quarter * kq, kq), kq), lane(kvh)],
            kvb.at[0:kq, W : 2 * W],
        )
        fetch("qg", qgain_hbm, qgain_v)
        fetch("kg", kgain_hbm, kgain_v)
        fetch("gg", ggate_hbm, ggate_v)
        fetch("lg", logits_hbm, logits_v)
        fetch("wg", wg_hbm, w13.at[:, 0:W])
        fetch("wu", wu_hbm, w13.at[:, W : 2 * W])
        load_d = []
        for k in range(2):
            for dx in range(nx):
                core = c if k == 0 else 1 - c
                col = ((x + dx) % nx) * 2 + core
                at = k * color + dx * W
                load_d.append(
                    pltpu.make_async_copy(
                        wd_hbm.at[:, lane(col)], wdp.at[:, at : at + W], wsem.at[k * nx + dx]
                    )
                )
                load_d[-1].start()
        fetch("wo", wout_hbm, wout_v)

    with jax.named_scope("slots"):
        local["routes"].wait()
        e_sub = lax.broadcasted_iota(jnp.int32, (nz, count), 0)
        r0 = routes_v[0:1, :]
        r1 = routes_v[1:2, :]
        named = jnp.where((r0 == e_sub) | (r1 == e_sub), 1.0, 0.0).astype(bf16)
        before = jnp.where(
            lax.broadcasted_iota(jnp.int32, (count, count), 0)
            < lax.broadcasted_iota(jnp.int32, (count, count), 1),
            1.0,
            0.0,
        ).astype(bf16)
        rank = jnp.dot(named, before, preferred_element_type=f32).astype(bf16)
        lo = lax.broadcasted_iota(jnp.int32, (nz * PAD, nz), 1) * PAD
        slot = lax.broadcasted_iota(jnp.int32, (nz * PAD, nz), 0)
        spread = jnp.where((slot >= lo) & (slot < lo + PAD), 1.0, 0.0).astype(bf16)
        slot_of = (lax.broadcasted_iota(jnp.int32, (nz * PAD, count), 0) % PAD).astype(f32)
        named_x = jnp.dot(spread, named, preferred_element_type=f32)
        rank_x = jnp.dot(spread, rank, preferred_element_type=f32)
        hit = (named_x > 0.5) & (jnp.abs(rank_x - slot_of) < 0.5)
        sslot[...] = jnp.where(hit, 1.0, 0.0)

    with jax.named_scope("norm"):
        local["rows"].wait()
        local["gain"].wait()
        wide = rows_v[...].astype(f32)
        inv = lax.rsqrt(jnp.mean(wide * wide, axis=-1, keepdims=True) + 1e-06)
        mine = rows_v[:, lane(t)].astype(f32) * inv * gain_v[:, lane(t)]
        sendb[...] = jnp.dot(
            sslot[...].astype(bf16), mine.astype(bf16), preferred_element_type=f32
        ).astype(bf16)

    with jax.named_scope("barrier"):
        pl.semaphore_wait(barrier, z + 5)

        def enter(j, carry):
            @pl.when(j < z)
            def _():
                pl.semaphore_signal(in_sem.at[z], inc=1, device_id={"ep": j}, device_id_type=MESH)

            return carry

        lax.fori_loop(0, nz, enter, 0)

    def block(i):
        return pl.ds(pl.multiple_of(i * PAD, PAD), PAD)

    def place(d):
        far = d // (nz // 2 + 1)
        return (1 - far) * (2 * d - 1) + far * 2 * (nz - d)

    def disp(j):
        p = place((z - j + nz) % nz)
        return remote(
            sendb.at[block(j)], recvb.at[block(p)], disp_s.at[j], disp_r.at[p], {"ep": j}
        )

    def disp_in(p):
        view = recvb.at[block(p)]
        return remote(view, view, disp_s.at[0], disp_r.at[p], {"ep": z})

    def turned(v, gain, first):
        n = v.shape[0]
        wide = v.astype(f32)
        v = wide * lax.rsqrt(jnp.mean(wide * wide, axis=-1, keepdims=True) + 1e-06) * gain
        p = first + lax.broadcasted_iota(jnp.int32, (n, W), 0)
        ln = lax.broadcasted_iota(jnp.int32, (n, W), 1)
        nf = HEAD_DIM // 4
        at = jnp.where(ln < 2 * nf, p // GRID_W, p % GRID_W).astype(f32)
        inverse = jnp.exp((ln % nf).astype(f32) * (-9.210340371976184 / nf))
        angle = at * inverse
        odd = (ln // nf) % 2 == 1
        h = jnp.where(odd, pltpu.roll(v, nf, 1), -pltpu.roll(v, W - nf, 1))
        return (v * jnp.cos(angle) + h * jnp.sin(angle)).astype(bf16)

    def qsend(m):
        return remote(qs.at[0], qs.at[m], q_s.at[m - 1], q_r.at[m - 1], {"tp": mates[m]})

    def kv_a(m):
        to = (z + 4 * m) % nz
        return remote(
            kvb.at[0:kq], kvb.at[pl.ds(pl.multiple_of(m * kq, kq), kq)], kva_s.at[m], kva_r.at[m], {"ep": to}
        )

    def kv_b(g):
        d = (0, 1, nz - 1, 2 + c * (nz - 4))[g]
        return remote(
            kvb.at[0:setrows],
            kvb.at[g * setrows : (g + 1) * setrows],
            kvb_s.at[g],
            kvb_r.at[g],
            {"ep": (z + d) % nz},
        )

    with jax.named_scope("rope_k"):
        local["k"].wait()
        local["kg"].wait()
        kvb[0:kq, 0:W] = turned(k_raw[...], kgain_v[...], z * qrows + quarter * kq)
        local["v"].wait()
        local["q"].wait()
        local["qg"].wait()
        qs[0] = turned(queries_v[...], qgain_v[...], z * qrows)
        for m in (2, 3, 1):
            qsend(m).start()
        recvb[0:PAD] = sendb[block(z)]
        prow = lax.broadcasted_iota(jnp.int32, (R, RP), 0)
        pcol = lax.broadcasted_iota(jnp.int32, (R, RP), 1)
        pack[...] = jnp.where(
            (prow // cap == pcol // PAD) & (prow % cap == pcol % PAD), 1.0, 0.0
        ).astype(bf16)
        urow = lax.broadcasted_iota(jnp.int32, (RP, R), 0)
        ucol = lax.broadcasted_iota(jnp.int32, (RP, R), 1)
        unpack[...] = jnp.where(
            (ucol // cap == urow // PAD) & (ucol % cap == urow % PAD), 1.0, 0.0
        ).astype(bf16)

    with jax.named_scope("dispatch"):

        def send_to(j, carry):
            @pl.when(j > z)
            def _():
                pl.semaphore_wait(in_sem.at[j], 1)

            @pl.when(j != z)
            def _():
                disp(j).start()

            d = (j - z + nz) % nz

            @pl.when((j != z) & (d % 4 == 0))
            def _():
                kv_a(d // 4).start()

            return carry

        lax.fori_loop(0, nz, send_to, 0)

    def at_rows(k):
        return pl.ds(pl.multiple_of(k * R, R), R)

    def ag(k, side, s):
        xo = (x + nx - (s - 1)) % nx if side == 0 else (x + s - 1) % nx
        cols = lane(xo * 2 + c)
        if s < half:
            part = at_rows(k)
        elif side == 0:
            part = pl.ds(pl.multiple_of(k * R, 16), up_rows)
        else:
            part = pl.ds(pl.multiple_of(k * R + up_rows, 16), R - up_rows)
        view = xall.at[part, cols]
        to = right if side == 0 else left
        return remote(view, view, ag_s.at[k, side, s - 1], ag_r.at[k, side, s - 1], {"tp": to})

    def dd_place(j):
        if j == 0:
            return x, None
        if j <= half - 1:
            return (x + nx - j) % nx, None
        if j <= 2 * half - 2:
            return (x + j - (half - 1)) % nx, None
        return (x + half) % nx, j - (2 * half - 1)

    def dd(k, j, mine_side):
        core = c if mine_side else 1 - c
        xo, far = dd_place(j)
        rows = at_rows(k)
        if far == 0:
            rows = pl.ds(pl.multiple_of(k * R, 16), up_rows)
        elif far == 1:
            rows = pl.ds(pl.multiple_of(k * R + up_rows, 16), R - up_rows)
        view = xall.at[rows, lane(xo * 2 + core)]
        return remote(view, view, dd_s.at[k, j], dd_r.at[k, j], {"tp": other})

    ndd = 2 * half + 1

    def arrive(k):
        for i in range(4):
            if i:
                disp_in(4 * k + i).wait_recv()
            else:

                @pl.when(k > 0)
                def _():
                    disp_in(4 * k).wait_recv()

        rows = pl.ds(pl.multiple_of(k * RP, RP), RP)
        packed = jnp.dot(pack[...], recvb[rows], preferred_element_type=f32)
        xall[at_rows(k), lane(t)] = packed.astype(bf16)
        ag(k, 0, 1).start()
        ag(k, 1, 1).start()
        dd(k, 0, True).start()

    def kv_second():
        with jax.named_scope("kv2"):
            for m in range(1, nset):
                kv_a(m).wait_recv()
            for g in (3, 1, 2):
                kv_b(g).start()

    def hop(k, s):
        for side in range(2):
            ag(k, side, s).wait_recv()
            if s < half:
                ag(k, side, s + 1).start()
                dd(k, s if side == 0 else half - 1 + s, True).start()
            else:
                dd(k, 2 * half - 1 + side, True).start()

    def prep():
        with jax.named_scope("prep"):
            sel = sslot[...]
            subs = lax.broadcasted_iota(jnp.int32, (nz, count), 0)
            first = jnp.where(routes_v[0:1, :] == subs, 1.0, 0.0).astype(bf16)
            low = lax.broadcasted_iota(jnp.int32, (nz * PAD, nz), 1) * PAD
            at = lax.broadcasted_iota(jnp.int32, (nz * PAD, nz), 0)
            expand = jnp.where((at >= low) & (at < low + PAD), 1.0, 0.0).astype(bf16)
            s_0 = jnp.where(jnp.dot(expand, first, preferred_element_type=f32) > 0.5, sel, 0.0)
            smat[0] = s_0.T.astype(bf16)
            smat[1] = (sel - s_0).T.astype(bf16)
            local["lg"].wait()
            local["gg"].wait()
            logits = logits_v[...]
            top = jnp.max(logits, axis=0, keepdims=True)
            ex = jnp.exp(logits - top)
            weights = ggate_v[...] * (ex / jnp.sum(ex, axis=0, keepdims=True))
            eye = lax.broadcasted_iota(jnp.int32, (count, count), 0) == lax.broadcasted_iota(
                jnp.int32, (count, count), 1
            )
            for e in range(2):
                col = jnp.sum(jnp.where(eye, weights[e : e + 1, :], 0.0), axis=1, keepdims=True)
                wcol[e] = jnp.broadcast_to(col, (count, W))
            local["wg"].wait()
            local["wu"].wait()
            local["wo"].wait()
            for cp in load_d:
                cp.wait()

    def pair(k):
        return remote(psend.at[k], precv.at[k], pr_s.at[k], pr_r.at[k], {"tp": other})

    def ffn(k):
        for j in range(ndd):
            dd(k, j, False).wait_recv()
        xk = xall[at_rows(k), :]
        h = jnp.dot(xk, w13[...], preferred_element_type=f32)
        g = h[:, 0:W]
        hidden = (g * jax.nn.sigmoid(g) * h[:, W : 2 * W]).astype(bf16)
        part = jnp.dot(hidden, wdp[...], preferred_element_type=f32).astype(bf16)
        psend[k] = part[:, color:]
        pairs[k] = part[:, :color].astype(f32)
        pair(k).start()

    def part_rows(side, s):
        if s > 1:
            return 0, R
        return (0, up_rows) if side == 0 else (up_rows, R)

    def rs(k, side, s):
        a, b = part_rows(side, s)
        to = right if side == 0 else left
        return remote(
            rs_send.at[k, side, s - 1, a:b],
            rs_recv.at[k, side, s - 1, a:b],
            rss_s.at[k, side, s - 1],
            rss_r.at[k, side, s - 1],
            {"tp": to},
        )

    def target(side, s):
        far = half + 1 - s
        return far if side == 0 else nx - far

    def rs_first(k):
        pair(k).wait_recv()
        pairs[k] = pairs[k] + precv[k].astype(f32)
        for side in range(2):
            a, b = part_rows(side, 1)
            at = target(side, 1) * W
            rs_send[k, side, 0, a:b] = pairs[k, a:b, at : at + W].astype(bf16)
            rs(k, side, 1).start()

    def rs_hop(k, s):
        for side in range(2):
            rs(k, side, s - 1).wait_recv()
            at = target(side, s) * W
            a, b = part_rows(side, s - 1)
            rs_send[k, side, s - 1, a:b] = (
                pairs[k, a:b, at : at + W] + rs_recv[k, side, s - 2, a:b].astype(f32)
            ).astype(bf16)
            if a > 0:
                rs_send[k, side, s - 1, 0:a] = pairs[k, 0:a, at : at + W].astype(bf16)
            if b < R:
                rs_send[k, side, s - 1, b:R] = pairs[k, b:R, at : at + W].astype(bf16)
            rs(k, side, s).start()

    def po(m):
        return remote(
            po_send.at[m - 1], po_recv.at[m - 1], po_s.at[m - 1], po_r.at[m - 1], {"tp": mates[m]}
        )

    def ls(m):
        return remote(
            ls_send.at[m - 1], ls_recv.at[m - 1], ls_s.at[m - 1], ls_r.at[m - 1], {"tp": mates[m]}
        )

    def attend(q):
        sc = lax.dot_general(
            q, kvb[:, 0:W], (((1,), (1,)), ((), ())), preferred_element_type=f32
        ) * (HEAD_DIM**-0.5)
        top = jnp.max(sc, axis=-1, keepdims=True)
        ex = jnp.exp(sc - top)
        total = jnp.sum(ex, axis=-1, keepdims=True)
        o = jnp.dot(ex.astype(bf16), kvb[:, W : 2 * W], preferred_element_type=f32) / total
        return o, jnp.broadcast_to(top + jnp.log(total), (qrows, W))

    def attend_all():
        with jax.named_scope("attwait"):
            for g in range(1, 4):
                kv_b(g).wait_recv()
            for m in (1, 2, 3):
                qsend(m).wait_recv()
        with jax.named_scope("attend"):
            for m in (2, 3, 1, 0):
                o, lse = attend(qs[m])
                if m:
                    po_send[m - 1] = o.astype(bf16)
                    ls_send[m - 1] = lse.T[0:8]
                    po(m).start()
                    ls(m).start()
                else:
                    o_own[...] = o
                    lse_own[...] = lse

    def oag(side, s):
        xo = (x + nx - (s - 1)) % nx if side == 0 else (x + s - 1) % nx
        hr = qrows // 2
        part = pl.ds(0, qrows) if s < half else pl.ds(side * hr, hr)
        view = heads.at[part, lane(xo * 2 + c)]
        to = right if side == 0 else left
        return remote(view, view, oag_s.at[side, s - 1], oag_r.at[side, s - 1], {"tp": to})

    def odd(j, mine_side):
        core = c if mine_side else 1 - c
        xo, far = dd_place(j)
        hr = qrows // 2
        part = pl.ds(0, qrows) if far is None else pl.ds(far * hr, hr)
        view = heads.at[part, lane(xo * 2 + core)]
        return remote(view, view, odd_s.at[j], odd_r.at[j], {"tp": other})

    def merge():
        with jax.named_scope("merge"):
            for m in (1, 2, 3):
                ls(m).wait_recv()
                po(m).wait_recv()
            parts = [lse_own[...]] + [
                jnp.broadcast_to(ls_recv[m, 0:1, :], (W, qrows)).T for m in range(3)
            ]
            top = jnp.maximum(jnp.maximum(parts[0], parts[1]), jnp.maximum(parts[2], parts[3]))
            den = jnp.exp(parts[0] - top)
            num = den * o_own[...]
            for m in range(3):
                wt = jnp.exp(parts[m + 1] - top)
                den = den + wt
                num = num + wt * po_recv[m].astype(f32)
            heads[:, lane(t)] = (num / den).astype(bf16)
            oag(0, 1).start()
            oag(1, 1).start()
            odd(0, True).start()

    def oag_hop(s):
        with jax.named_scope(f"oag{s}"):
            for side in range(2):
                oag(side, s).wait_recv()
                if s < half:
                    oag(side, s + 1).start()
                    odd(s if side == 0 else half - 1 + s, True).start()
                else:
                    odd(2 * half - 1 + side, True).start()

    def ret(d, p):
        return remote(
            ret_send.at[block(p)],
            ret_recv.at[block(z)],
            ret_s.at[d],
            ret_r.at[(nz - d) % nz],
            {"ep": (z + d) % nz},
        )

    def ret_in(d):
        view = ret_recv.at[block((z + d) % nz)]
        return remote(view, view, ret_s.at[d], ret_r.at[d], {"ep": (z + d) % nz})

    def back(k):
        for side in range(2):
            rs(k, side, half).wait_recv()
            a, b = part_rows(side, half)
            pairs[k, a:b, 0:W] = pairs[k, a:b, 0:W] + rs_recv[k, side, half - 1, a:b].astype(f32)
        y = pairs[k, :, 0:W].astype(bf16)
        rows = pl.ds(pl.multiple_of(k * RP, RP), RP)
        ret_send[rows] = jnp.dot(unpack[...], y, preferred_element_type=f32).astype(bf16)
        for i in range(4):
            d = 2 * k + (i + 1) // 2 if i % 2 else (nz - 2 * k - i // 2) % nz
            if i:
                ret(d, 4 * k + i).start()
            else:

                @pl.when(k > 0)
                def _(d=d):
                    ret(d, 4 * k).start()

    stages = [("arrive", arrive)]
    stages += [(f"hop{s}", functools.partial(hop, s=s)) for s in range(1, half + 1)]
    stages += [("ffn", ffn), ("rs1", rs_first)]
    stages += [(f"rs{s}", functools.partial(rs_hop, s=s)) for s in range(2, half + 1)]
    stages += [("back", back)]
    steps = nchunk + len(stages) - 1
    events = [(1, prep), (3, kv_second), (6, attend_all), (8, merge)]
    events += [(8 + s, functools.partial(oag_hop, s)) for s in range(1, half + 1)]

    def wave(step, carry):
        for n in range(len(stages) - 1, -1, -1):
            name, run = stages[n]

            @pl.when((step >= n) & (step < n + nchunk))
            def _(n=n, name=name, run=run):
                with jax.named_scope(name):
                    run(step - n)

        for at, run in events:
            pl.when(step == min(at, steps - 1))(run)
        return carry

    lax.fori_loop(0, steps, wave, 0)
    ret_recv[block(z)] = ret_send[0:PAD]

    with jax.named_scope("project"):
        for j in range(ndd):
            odd(j, False).wait_recv()
        attn_ref[...] = jnp.dot(heads[...], wout_v[...], preferred_element_type=f32).astype(bf16)

    with jax.named_scope("retwait"):
        for d in order[1:]:
            ret_in(d).wait_recv()
    with jax.named_scope("combine"):
        table = ret_recv[...]
        p0 = jnp.dot(smat[0], table, preferred_element_type=f32)
        p1 = jnp.dot(smat[1], table, preferred_element_type=f32)
        out_ref[...] = (wcol[0] * p0 + wcol[1] * p1).astype(bf16)

    with jax.named_scope("drain"):

        def sent(j, carry):
            @pl.when(j != z)
            def _():
                disp(j).wait_send()

            return carry

        lax.fori_loop(0, nz, sent, 0)
        for d in range(1, nz):
            ret(d, 0).wait_send()
        for m in range(1, nset):
            kv_a(m).wait_send()
        for m in (1, 2, 3):
            kv_b(m).wait_send()
            qsend(m).wait_send()
            po(m).wait_send()
            ls(m).wait_send()
        for j in range(ndd):
            odd(j, True).wait_send()
        for side in range(2):
            for s in range(1, half + 1):
                oag(side, s).wait_send()

        def drain(k, carry):
            for side in range(2):
                for s in range(1, half + 1):
                    ag(k, side, s).wait_send()
                    rs(k, side, s).wait_send()
            for j in range(ndd):
                dd(k, j, True).wait_send()
            pair(k).wait_send()
            return carry

        lax.fori_loop(0, nchunk, drain, 0)


def fused(mesh, queries, keys, values, qg, kg, wo, rows, routes, gg, lg, gain, wgate, wup, wdown):
    nz, nt = mesh.shape["ep"], mesh.shape["tp"]
    count, width = rows.shape
    qrows = queries.shape[0]
    kq = qrows // GROUP
    nx = nt // 2
    half = nx // 2
    cap = 3 * count // nz
    k = nz // 4
    R = 4 * cap
    color = nx * W
    ndd = 2 * half + 1
    dma = pltpu.SemaphoreType.DMA
    V = pltpu.VMEM
    shapes = dict(
        queries_v=V((qrows, W), bf16),
        k_raw=V((kq, W), bf16),
        kvb=V((nz * kq, 2 * W), bf16),
        qs=V((GROUP, qrows, W), bf16),
        qgain_v=V((1, W), f32),
        kgain_v=V((1, W), f32),
        wout_v=V((nt * W, W), bf16),
        o_own=V((qrows, W), f32),
        lse_own=V((qrows, W), f32),
        po_send=V((3, qrows, W), bf16),
        po_recv=V((3, qrows, W), bf16),
        ls_send=V((3, 8, qrows), f32),
        ls_recv=V((3, 8, qrows), f32),
        heads=V((qrows, nt * W), bf16),
        rows_v=V((count, width), bf16),
        routes_v=V((2, count), jnp.int32),
        ggate_v=V((1, count), f32),
        logits_v=V((2, count), f32),
        gain_v=V((1, width), f32),
        w13=V((width, 2 * W), bf16),
        wdp=V((W, width), bf16),
        sendb=V((nz * PAD, W), bf16),
        recvb=V((nz * PAD, W), bf16),
        xall=V((k * R, width), bf16),
        pairs=V((k, R, color), f32),
        psend=V((k, R, color), bf16),
        precv=V((k, R, color), bf16),
        rs_send=V((k, 2, half, R, W), bf16),
        rs_recv=V((k, 2, half, R, W), bf16),
        ret_send=V((nz * PAD, W), bf16),
        ret_recv=V((nz * PAD, W), bf16),
        sslot=V((nz * PAD, count), f32),
        smat=V((2, count, nz * PAD), bf16),
        wcol=V((2, count, W), f32),
        lsem=dma((16,)),
        wsem=dma((2 * nx,)),
        disp_s=dma((nz,)),
        disp_r=dma((nz,)),
        ag_s=dma((k, 2, half)),
        ag_r=dma((k, 2, half)),
        dd_s=dma((k, ndd)),
        dd_r=dma((k, ndd)),
        pr_s=dma((k,)),
        pr_r=dma((k,)),
        rss_s=dma((k, 2, half)),
        rss_r=dma((k, 2, half)),
        ret_s=dma((nz,)),
        ret_r=dma((nz,)),
        q_s=dma((3,)),
        q_r=dma((3,)),
        kva_s=dma((k,)),
        kva_r=dma((k,)),
        kvb_s=dma((4,)),
        kvb_r=dma((4,)),
        po_s=dma((3,)),
        po_r=dma((3,)),
        ls_s=dma((3,)),
        ls_r=dma((3,)),
        oag_s=dma((2, half)),
        oag_r=dma((2, half)),
        odd_s=dma((ndd,)),
        odd_r=dma((ndd,)),
        in_sem=pltpu.SemaphoreType.REGULAR((nz,)),
        pack=V((R, 4 * PAD), bf16),
        unpack=V((4 * PAD, R), bf16),
    )
    vmem = pl.BlockSpec(memory_space=pltpu.VMEM)
    hbm = pl.BlockSpec(memory_space=pl.ANY)
    return pl.pallas_call(
        functools.partial(fused_kernel, nz, nt),
        out_shape=(
            jax.ShapeDtypeStruct((qrows, W), bf16),
            jax.ShapeDtypeStruct((count, W), bf16),
        ),
        in_specs=[hbm] * 14,
        out_specs=(vmem, vmem),
        scratch_shapes=[shapes[n] for n in SCRATCH],
        compiler_params=pltpu.CompilerParams(collective_id=0, has_side_effects=True),
        name="fused",
    )(
        queries,
        keys,
        values,
        qg.reshape(1, -1),
        kg.reshape(1, -1),
        wo,
        rows,
        routes.T,
        gg.reshape(1, -1),
        lg.T,
        gain.reshape(1, -1),
        wgate[0],
        wup[0],
        wdown[0],
    )


def solution(mesh):
    placed = (
        P(("grp", "ep"), "tp"),
        P(("grp", "ep"), None),
        P(("grp", "ep"), None),
        P(),
        P(),
        P(None, "tp"),
        P(("grp", "ep"), None),
        P(("grp", "ep"), None),
        P(("grp", "ep")),
        P(("grp", "ep"), None),
        P(),
        P("ep", None, "tp"),
        P("ep", None, "tp"),
        P("ep", "tp", None),
    )
    return jax.shard_map(
        functools.partial(fused, mesh),
        mesh=mesh,
        in_specs=placed,
        out_specs=(P(("grp", "ep"), "tp"), P(("grp", "ep"), "tp")),
        check_vma=False,
    )
```

time: 256 us -> 119 us (0.46)
  the two profiles are of different devices: /device:TPU:80 before, /device:TPU:66 now
where the time goes in v2:
time: 119 us
  Pallas kernels  116 us (97%)
  local copies, waits for them, and re-layouts  2.11 us (2%)
    pallas_call x1, Pallas kernels, fused(): pl.pallas_call(functools.partial(fused_kernel, nz, nt), out_shape=(jax.Sh...  116 us

profile of v2, /device:TPU:66, one launch (start us, length us, event | category | flops | bytes accessed | tf_op | source)
XLA Modules:
  0.0 118.9 jit_solution(17836879378777843127)
XLA Ops:
  0.6 116.2 %fused.1 = (bf16[256,128]{1,0:T(8,128)(2,1)}, bf16[192,128]{1,0:T(8,128)(2,1)}) custom-call(bf16[256,128]{1,0:T(8,128)(2,1)} %refs_0_.1, bf16[256,512]{1,0:T(8,128)(2,1)} %refs_1_.1, bf16[256,512]{1,0:T(8,128)(2,1)} %refs_2_.1, f32[1,128]{1,0:T(1,128)} %bitcast.16, f32[1,128]{1,0:T(1,128)} %bitcast.17, bf16[2048,128]{1,0:T(8,128)(2,1)} %refs_5_.1, ...), custom_call_target="tpu_custom_call" | custom-call | tf_op jit(solution)/shard_map/fused/pallas_call | solution.py:768
  116.8 0.0 copy-start
  116.8 1.5 %copy.18 = bf16[256,128]{1,0:T(8,128)(2,1)} copy(bf16[256,128]{1,0:T(8,128)(2,1)} %get-tuple-element.4) | data formatting | bytes 131072
  118.3 0.0 copy-done
  118.3 0.6 copy.19
Async XLA Ops:
  116.8 1.5 %copy-start = (bf16[192,128]{1,0:T(8,128)(2,1)S(1)}, bf16[192,128]{1,0:T(8,128)(2,1)}, u32[]{:S(2)}) copy-start(bf16[192,128]{1,0:T(8,128)(2,1)} %get-tuple-element.5) | copy-start | bytes 147460
